TPU v7x, 512 devices: a whole 4x4x16 slice. The times are simulated.
512 devices in a mesh: ep: 32 (over z, core), tp: 16 (over y, x).
Axes of the slice: x: 4, y: 4, z: 16, core: 2. Of those that a mesh axis runs over, the one named last changes fastest.
Arguments:
- tokens: bfloat16 [512, 2048], P('ep'), may hold values from -6 to 6
- attn_gain: float32 [2048], replicated, may hold values from 0.1 to 1.9
- query_weight: bfloat16 [2048, 2048], P('ep', 'tp'), may hold values from -0.125 to 0.125
- key_weight: bfloat16 [2048, 2048], P('ep', 'tp'), may hold values from -0.125 to 0.125
- value_weight: bfloat16 [2048, 2048], P('ep', 'tp'), may hold values from -0.125 to 0.125
- forget_weight: bfloat16 [2048, 16], P(None, 'tp'), may hold values from -0.125 to 0.125
- forget_bias: float32 [16], P('tp'), may hold values from -1 to 2
- cache_keys: bfloat16 [512, 16, 384, 128], P('ep', 'tp'), may hold values from -240 to 240
- cache_values: bfloat16 [512, 16, 384, 128], P('ep', 'tp'), may hold values from -6 to 6
- cache_gates: float32 [512, 16, 384], P('ep', 'tp'), may hold values from -768 to 0, as said below
- lengths: int32 [512], P('ep'), may hold values from 1 to 384
- output_weight: bfloat16 [2048, 2048], P('tp', 'ep'), may hold values from -0.125 to 0.125
- ffn_gain: float32 [2048], replicated, may hold values from 0.1 to 1.9
- dense_gate_proj: bfloat16 [2048, 2048], P('ep', 'tp'), may hold values from -0.125 to 0.125
- dense_up_proj: bfloat16 [2048, 2048], P('ep', 'tp'), may hold values from -0.125 to 0.125
- dense_down_proj: bfloat16 [2048, 2048], P('tp', 'ep'), may hold values from -0.125 to 0.125
- dense_mix: bfloat16 [2048], replicated, may hold values from -0.125 to 0.125
- expert_ids: int32 [512, 2], P('ep'), may hold values from 0 to 31, as said below
- group_prob: float32 [512], P('ep'), may hold values from 0.25 to 1
- pair_prob: float32 [512, 2], P('ep'), may hold values from 0.05 to 1
- expert_gate: bfloat16 [32, 2048, 2048], P('ep', None, 'tp'), may hold values from -0.125 to 0.125
- expert_up: bfloat16 [32, 2048, 2048], P('ep', None, 'tp'), may hold values from -0.125 to 0.125
- expert_down: bfloat16 [32, 2048, 2048], P('ep', 'tp'), may hold values from -0.125 to 0.125
Outputs:
- mixed_out: bfloat16 [512, 2048], P('ep')
Inputs may be any that keep to these rules, and one draw needn't show every extreme that they name: `expert_ids`: each row names two different experts of one group, the groups being 4 runs of consecutive ids. In each aligned block of 16 rows (the rows of one index of ep) no expert is named more than 2 times, and some expert exactly 2 times. `cache_gates`: along positions the values never rise.
All inputs are finite; a program needn't handle non-finite values.
Results may differ from a plain program's by a relative error of at most 0.014.
Values may be sent and summed in bfloat16 or wider, within the bound.
No kernel may reach another device: no remote copies, remote signals or barrier semaphores. Data moves between devices by JAX's collectives and lax.ppermute only.
A program may use at most 64 MiB of HBM per device.

v0:
```python
import math
import jax
import jax.numpy as jnp
from jax import lax
from jax.sharding import Mesh
from jax.sharding import PartitionSpec as P

EP = ("ep_0", "ep_1")
EPSILON = 1e-06


def sent_together(arrays, axis, dim, along):
    widths = [a.shape[along] for a in arrays]
    both = jnp.concatenate(arrays, axis=along)
    filled = lax.all_gather(both, axis, axis=dim, tiled=True)
    return tuple(jnp.split(filled, [sum(widths[:k]) for k in range(1, len(widths))], axis=along))


def from_everyone(array, axis):
    copies = jnp.broadcast_to(array, (lax.axis_size(axis), *array.shape))
    return lax.all_to_all(copies, axis, split_axis=0, concat_axis=0, tiled=True)


def laid_out(pieces, dim):
    lengths = list(pieces.shape[1:])
    lengths[dim] *= pieces.shape[0]
    return jnp.moveaxis(pieces, 0, dim).reshape(lengths)


def collect(array, axis, dim):
    pieces = from_everyone(array, axis)
    return laid_out(pieces, dim)


def taken_together(array, axis):
    everything = from_everyone(array, axis)
    return jnp.sum(everything.astype(jnp.float32), axis=0)


def gather_in_order(array, axes, sequence):
    pieces = array[None]
    for k in sequence:
        pieces = lax.all_gather(pieces, axes[k], axis=0, tiled=True)
    held = [lax.axis_size(axes[k]) for k in reversed(sequence)]
    pieces = pieces.reshape(*held, *array.shape)
    turned = sorted(range(len(sequence)), key=lambda place: sequence[len(sequence) - 1 - place])
    return pieces.transpose(*turned, *range(len(sequence), pieces.ndim)).reshape(-1, *array.shape)


def gathered_by_axis(array, axes, sequence, dim):
    return laid_out(gather_in_order(array, axes, sequence), dim)


def rms_scale(values, norm_gain):
    widened = values.astype(jnp.float32)
    return (
        widened
        * lax.rsqrt(jnp.mean(widened * widened, axis=-1, keepdims=True) + EPSILON)
        * norm_gain
    )


def attend(queries, keys_new, values_new, key_cache, value_cache, gate_cache, lengths, log_forget):
    cache_span = key_cache.shape[2]
    score_scale = 1.0 / math.sqrt(key_cache.shape[3])
    positions = jnp.arange(cache_span, dtype=jnp.int32)
    live_mask = positions[None, :] < lengths[:, None]
    last_mask = positions[None, :] == lengths[:, None] - 1
    last_gate = jnp.sum(jnp.where(last_mask[:, None, :], gate_cache, 0.0), axis=-1)
    gate_now = last_gate + log_forget
    scores = (
        jnp.einsum("shd,shpd->shp", queries, key_cache, preferred_element_type=jnp.float32)
        * score_scale
    )
    scores = scores + gate_now[:, :, None] - gate_cache
    scores = jnp.where(live_mask[:, None, :], scores, -jnp.inf)
    own_score = (
        jnp.sum(queries.astype(jnp.float32) * keys_new.astype(jnp.float32), axis=-1) * score_scale
    )
    row_top = jnp.maximum(jnp.max(scores, axis=-1), own_score)
    raised = jnp.exp(scores - row_top[:, :, None])
    own_raised = jnp.exp(own_score - row_top)
    totals = jnp.sum(raised, axis=-1) + own_raised
    weights_low = (raised / totals[:, :, None]).astype(jnp.bfloat16)
    own_prob = (own_raised / totals).astype(jnp.bfloat16)
    attended = jnp.einsum(
        "shp,shpd->shd", weights_low, value_cache, preferred_element_type=jnp.float32
    )
    attended = attended + own_prob.astype(jnp.float32)[:, :, None] * values_new.astype(jnp.float32)
    return attended.astype(jnp.bfloat16)


def column_fold(source, pieces):
    return tuple(
        (
            jnp.dot(source, weight_piece, preferred_element_type=jnp.float32)
            for weight_piece in pieces
        )
    )


def right_product(left_rows, weight_piece):
    return jnp.dot(left_rows, weight_piece, preferred_element_type=jnp.float32)


def shards(
    tokens,
    attn_gain,
    query_weight,
    key_weight,
    value_weight,
    forget_weight,
    forget_bias,
    cache_keys,
    cache_values,
    cache_gates,
    lengths,
    output_weight,
    ffn_gain,
    dense_gate_proj,
    dense_up_proj,
    dense_down_proj,
    dense_mix,
    expert_ids,
    group_prob,
    pair_prob,
    expert_gate,
    expert_up,
    expert_down,
):
    seq_count = tokens.shape[0]
    head_count = cache_keys.shape[1]
    head_size = cache_keys.shape[3]
    normed = rms_scale(tokens, attn_gain).astype(jnp.bfloat16)
    projected = column_fold(
        normed, sent_together((query_weight, key_weight, value_weight), EP, 0, 1)
    )
    queries = projected[0].astype(jnp.bfloat16).reshape(seq_count, head_count, head_size)
    keys_new = projected[1].astype(jnp.bfloat16).reshape(seq_count, head_count, head_size)
    values_new = projected[2].astype(jnp.bfloat16).reshape(seq_count, head_count, head_size)
    log_forget = jax.nn.log_sigmoid(
        jnp.dot(normed, forget_weight, preferred_element_type=jnp.float32) + forget_bias
    )
    attended = attend(
        queries, keys_new, values_new, cache_keys, cache_values, cache_gates, lengths, log_forget
    )
    attended = attended.reshape(seq_count, head_count * head_size)
    head_terms = right_product(attended, collect(output_weight, EP, 1))
    mixed_heads = taken_together(head_terms.astype(jnp.bfloat16), "tp").astype(jnp.float32)
    residual = (tokens.astype(jnp.float32) + mixed_heads).astype(jnp.bfloat16)
    ffn_in = rms_scale(residual, ffn_gain).astype(jnp.bfloat16)
    dense_parts = column_fold(ffn_in, sent_together((dense_gate_proj, dense_up_proj), EP, 0, 1))
    dense_hidden = (jax.nn.silu(dense_parts[0]) * dense_parts[1]).astype(jnp.bfloat16)
    dense_terms = right_product(dense_hidden, gathered_by_axis(dense_down_proj, EP, (0, 1), 1))
    mix = jax.nn.sigmoid(jnp.dot(ffn_in, dense_mix, preferred_element_type=jnp.float32))
    expert_count = lax.axis_size(EP) * expert_gate.shape[0]
    capacity = 4 * seq_count // expert_count
    slot_total = expert_count * capacity
    picks = expert_ids.reshape(-1)
    expert_grid = jnp.arange(expert_count, dtype=jnp.int32)
    pick_onehot = (picks[:, None] == expert_grid[None, :]).astype(jnp.int32)
    earlier = jnp.cumsum(pick_onehot, axis=0) - pick_onehot
    slot_rank = jnp.sum(earlier * pick_onehot, axis=1)
    destination = (picks * capacity + slot_rank).reshape(seq_count, 2)
    slot_grid = jnp.arange(slot_total, dtype=jnp.int32)
    select_first = (destination[:, 0:1] == slot_grid[None, :]).astype(jnp.bfloat16)
    select_second = (destination[:, 1:2] == slot_grid[None, :]).astype(jnp.bfloat16)
    selector = select_first + select_second
    outbound = jnp.einsum("sk,sd->kd", selector, ffn_in, preferred_element_type=jnp.float32)
    outbound = outbound.astype(jnp.bfloat16).reshape(expert_count, capacity, ffn_in.shape[1])
    arrived = lax.all_to_all(outbound, EP, split_axis=0, concat_axis=0, tiled=True)
    sources, slots_now, feature = arrived.shape
    row_data = arrived.reshape(sources * slots_now, feature)
    gate_part = jnp.dot(row_data, expert_gate[0], preferred_element_type=jnp.float32)
    up_part = jnp.dot(row_data, expert_up[0], preferred_element_type=jnp.float32)
    expert_hidden = (jax.nn.silu(gate_part) * up_part).astype(jnp.bfloat16)
    partial_out = jnp.dot(expert_hidden, expert_down[0], preferred_element_type=jnp.float32)
    returned = lax.all_to_all(
        partial_out.reshape(sources, slots_now, feature).astype(jnp.bfloat16),
        EP,
        split_axis=0,
        concat_axis=0,
        tiled=True,
    ).astype(jnp.float32)
    returned = returned.reshape(slot_total, ffn_in.shape[1])
    routes = group_prob[:, None] * pair_prob / jnp.sum(pair_prob, axis=1, keepdims=True)
    first_back = returned[destination[:, 0]]
    second_back = returned[destination[:, 1]]
    side_total = (
        routes[:, 0:1] * first_back + routes[:, 1:2] * second_back + mix[:, None] * dense_terms
    )
    side_total = taken_together(side_total.astype(jnp.bfloat16), "tp").astype(jnp.float32)
    result = residual.astype(jnp.float32) + side_total
    return result.astype(jnp.bfloat16)


def solution(mesh):
    finer = Mesh(mesh.devices.reshape(16, 2, mesh.shape["tp"]), ("ep_0", "ep_1", "tp"))
    in_specs = (
        P(EP, None),
        P(),
        P(EP, "tp"),
        P(EP, "tp"),
        P(EP, "tp"),
        P(None, "tp"),
        P("tp"),
        P(EP, "tp", None, None),
        P(EP, "tp", None, None),
        P(EP, "tp", None),
        P(EP),
        P("tp", EP),
        P(),
        P(EP, "tp"),
        P(EP, "tp"),
        P("tp", EP),
        P(),
        P(EP, None),
        P(EP),
        P(EP, None),
        P(EP, None, "tp"),
        P(EP, None, "tp"),
        P(EP, "tp", None),
    )
    out_specs = P(EP, None)
    return jax.shard_map(
        shards, mesh=finer, in_specs=in_specs, out_specs=out_specs, check_vma=False
    )
```

profile of v0, /device:TPU:1, one launch (start us, length us, event | category | flops | bytes accessed | tf_op | source)
XLA Modules:
  0.0 240.2 jit_solution(12965718424162420117)
XLA Ops:
  6.6 1.5 pad_maximum_fusion
  8.1 1.6 broadcast_in_dim.17
  9.7 16.7 %all-to-all-start = ((bf16[32,128,64]{1,2,0:T(8,128)(2,1)}), bf16[32,128,64]{1,2,0:T(8,128)(2,1)S(1)}, u32[]{:S(2)}, u32[]{:S(2)}) async-start(bf16[32,128,64]{1,2,0:T(8,128)(2,1)} %broadcast_in_dim.17), calls=%async_computation | async-start | bytes 1048576 | tf_op jit(solution)/shard_map/all_to_all | solution.py:21
  27.8 63.6 %all-gather.4.cloned.1.call-done = bf16[2048,384]{1,0:T(8,128)(2,1)} async-done(((bf16[64,384]{1,0:T(8,128)(2,1)}), bf16[2048,384]{1,0:T(8,128)(2,1)}) %all-gather.4.cloned.1.call-update) | async-done | bytes 1572880 | tf_op jit(solution)/shard_map/all_gather | solution.py:15
  91.4 1.4 convolution_convert_fusion.5
  92.8 1.4 fusion.14
  94.2 0.6 fusion.4
  96.0 1.5 convolution_convert_fusion.2
  97.5 1.1 broadcast_in_dim.18
  98.6 6.6 %all-to-all-start.1 = ((bf16[16,16,2048]{2,1,0:T(8,128)(2,1)}), bf16[16,16,2048]{2,1,0:T(8,128)(2,1)S(1)}, u32[]{:S(2)}, u32[]{:S(2)}) async-start(bf16[16,16,2048]{2,1,0:T(8,128)(2,1)} %broadcast_in_dim.18), calls=%async_computation.1 | async-start | bytes 2097152 | tf_op jit(solution)/shard_map/all_to_all | solution.py:21
  106.0 15.7 %all-to-all-done.1 = bf16[16,16,2048]{2,1,0:T(8,128)(2,1)S(1)} async-done(((bf16[16,16,2048]{2,1,0:T(8,128)(2,1)}), bf16[16,16,2048]{2,1,0:T(8,128)(2,1)S(1)}, u32[]{:S(2)}, u32[]{:S(2)}) %all-to-all-start.1) | async-done | bytes 1048608 | tf_op jit(solution)/shard_map/all_to_all | solution.py:21
  122.3 0.9 reshape.216
  123.2 10.1 %all-to-all-start.2 = ((bf16[32,2,2048]{2,1,0:T(2,128)(2,1)}), bf16[32,2,2048]{2,1,0:T(2,128)(2,1)S(1)}, u32[]{:S(2)}, u32[]{:S(2)}) async-start(bf16[32,2,2048]{2,1,0:T(2,128)(2,1)} %reshape.216), calls=%async_computation.2 | async-start | bytes 524288 | tf_op jit(solution)/shard_map/all_to_all | solution.py:171
  134.0 32.8 %all-gather = bf16[2048,64]{0,1:T(8,128)(2,1)S(1)} all-gather(bf16[128,64]{0,1:T(8,128)(2,1)S(1)} %copy-done.6), channel_id=2, replica_groups=mesh['ep_0'=16,'ep_1'=2,'tp'=16] {'ep_0'}, dimensions={0}, use_global_device_ids=true | all-gather | bytes 278528 | tf_op jit(solution)/shard_map/all_gather | solution.py:43
  166.9 7.8 %all_gather.15 = bf16[32,128,64]{1,0,2:T(8,128)(2,1)S(1)} all-gather(bf16[16,128,64]{1,0,2:T(8,128)(2,1)S(1)} %bitcast.83), channel_id=1, replica_groups=mesh['ep_0'=16,'ep_1'=2,'tp'=16] {'ep_1'}, dimensions={0}, use_global_device_ids=true | all-gather | bytes 786432 | tf_op jit(solution)/shard_map/all_gather | solution.py:43
  175.3 1.3 fusion.6
  176.8 1.0 copy.64
  177.8 10.6 %all-to-all-start.3 = ((bf16[32,2,2048]{2,1,0:T(2,128)(2,1)}), bf16[32,2,2048]{2,1,0:T(2,128)(2,1)S(1)}, u32[]{:S(2)}, u32[]{:S(2)}) async-start(bf16[32,2,2048]{2,1,0:T(2,128)(2,1)} %copy.64), calls=%async_computation.3 | async-start | bytes 524288 | tf_op jit(solution)/shard_map/all_to_all | solution.py:178
  188.7 17.2 %all-gather.6.cloned.1.call-done = bf16[2048,256]{1,0:T(8,128)(2,1)} async-done(((bf16[64,256]{1,0:T(8,128)(2,1)}), bf16[2048,256]{1,0:T(8,128)(2,1)}) %all-gather.6.cloned.1.call-update) | async-done | bytes 1048592 | tf_op jit(solution)/shard_map/all_gather | solution.py:15
  205.9 1.3 fusion.23
  207.2 3.8 %all-to-all-done.3 = bf16[32,2,2048]{2,1,0:T(2,128)(2,1)S(1)} async-done(((bf16[32,2,2048]{2,1,0:T(2,128)(2,1)}), bf16[32,2,2048]{2,1,0:T(2,128)(2,1)S(1)}, u32[]{:S(2)}, u32[]{:S(2)}) %all-to-all-start.3) | async-done | bytes 262176 | tf_op jit(solution)/shard_map/all_to_all | solution.py:178
  212.3 1.5 fusion.1
  213.9 18.7 %all_to_all.25 = bf16[16,16,2048]{2,1,0:T(8,128)(2,1)S(1)} all-to-all(bf16[16,16,2048]{2,1,0:T(8,128)(2,1)S(1)} %broadcast_in_dim.20), channel_id=1, replica_groups=mesh['ep_0'=16,'ep_1'=2,'tp'=16] {'tp'}, dimensions={0} | all-to-all | bytes 2097152 | tf_op jit(solution)/shard_map/all_to_all | solution.py:21
  232.8 0.6 fusion.40
  (81 shorter events, 6.5 us)
Async XLA Ops:
  6.5 87.7 %copy-start = (bf16[16,1,384,128]{3,2,1,0:T(8,128)(2,1)S(1)}, bf16[16,1,384,128]{3,2,1,0:T(8,128)(2,1)}, u32[]{:S(2)}) copy-start(bf16[16,1,384,128]{3,2,1,0:T(8,128)(2,1)} %param.30) | copy-start | bytes 4718596
  6.5 20.6 %copy-start.1 = (bf16[16,2048]{1,0:T(8,128)(2,1)S(1)}, bf16[16,2048]{1,0:T(8,128)(2,1)}, u32[]{:S(2)}) copy-start(bf16[16,2048]{1,0:T(8,128)(2,1)} %param.23) | copy-start | bytes 196612
  6.5 20.7 %copy-start.13 = (s32[16]{0:T(128)S(1)}, s32[16]{0:T(128)}, u32[]{:S(2)}) copy-start(s32[16]{0:T(128)} %param.33) | copy-start | bytes 196
  6.5 20.8 %copy-start.4 = (f32[16,1,384]{2,1,0:T(1,128)S(1)}, f32[16,1,384]{2,1,0:T(1,128)}, u32[]{:S(2)}) copy-start(f32[16,1,384]{2,1,0:T(1,128)} %param.32) | copy-start | bytes 73732
  6.5 21.0 %copy-start.9 = (f32[2048]{0:T(1024)S(1)}, f32[2048]{0:T(1024)}, u32[]{:S(2)}) copy-start(f32[2048]{0:T(1024)} %param.24) | copy-start | bytes 24580
  6.5 21.1 %copy-start.16 = (bf16[2048,1]{0,1:T(2,128)(2,1)S(1)}, bf16[2048,1]{0,1:T(2,128)(2,1)}, u32[]{:S(2)}) copy-start(bf16[2048,1]{0,1:T(2,128)(2,1)} %param.28) | copy-start | bytes 12292
  6.6 84.8 %all-gather.4.cloned.1.call-start = ((), (), s32[]{:S(2)}) async-start(), calls=%async_computation.5 | async-start | bytes 1622016 | tf_op jit(solution)/shard_map/all_gather | solution.py:15
  9.7 86.3 %all-to-all-start = ((bf16[32,128,64]{1,2,0:T(8,128)(2,1)}), bf16[32,128,64]{1,2,0:T(8,128)(2,1)S(1)}, u32[]{:S(2)}, u32[]{:S(2)}) async-start(bf16[32,128,64]{1,2,0:T(8,128)(2,1)} %broadcast_in_dim.17), calls=%async_computation | async-start | bytes 1048576 | tf_op jit(solution)/shard_map/all_to_all | solution.py:21
  91.4 4.2 %copy-start.15 = (bf16[16,1,384,128]{3,2,1,0:T(8,128)(2,1)S(1)}, bf16[16,1,384,128]{3,2,1,0:T(8,128)(2,1)}, u32[]{:S(2)}) copy-start(bf16[16,1,384,128]{3,2,1,0:T(8,128)(2,1)} %param.31) | copy-start | bytes 4718596
  97.5 7.7 %copy-start.11 = (s32[16,2]{0,1:T(2,128)S(1)}, s32[16,2]{0,1:T(2,128)}, u32[]{:S(2)}) copy-start(s32[16,2]{0,1:T(2,128)} %param.40) | copy-start | bytes 388
  98.6 23.3 %copy-start.5 = (f32[2048]{0:T(1024)S(1)}, f32[2048]{0:T(1024)}, u32[]{:S(2)}) copy-start(f32[2048]{0:T(1024)} %param.35) | copy-start | bytes 24580
  98.6 23.0 %all-to-all-start.1 = ((bf16[16,16,2048]{2,1,0:T(8,128)(2,1)}), bf16[16,16,2048]{2,1,0:T(8,128)(2,1)S(1)}, u32[]{:S(2)}, u32[]{:S(2)}) async-start(bf16[16,16,2048]{2,1,0:T(8,128)(2,1)} %broadcast_in_dim.18), calls=%async_computation.1 | async-start | bytes 2097152 | tf_op jit(solution)/shard_map/all_to_all | solution.py:21
  105.2 28.1 %copy-start.7 = (bf16[64,128]{1,0:T(8,128)(2,1)S(1)}, bf16[64,128]{1,0:T(8,128)(2,1)}, u32[]{:S(2)}) copy-start(bf16[64,128]{1,0:T(8,128)(2,1)} %param.37) | copy-start | bytes 49156
  105.2 28.1 %copy-start.8 = (bf16[64,128]{1,0:T(8,128)(2,1)S(1)}, bf16[64,128]{1,0:T(8,128)(2,1)}, u32[]{:S(2)}) copy-start(bf16[64,128]{1,0:T(8,128)(2,1)} %param.36) | copy-start | bytes 49156
  105.3 28.7 %copy-start.10 = (bf16[2048]{0:T(1024)(128)(2,1)S(1)}, bf16[2048]{0:T(1024)(128)(2,1)}, u32[]{:S(2)}) copy-start(bf16[2048]{0:T(1024)(128)(2,1)} %param.39) | copy-start | bytes 12292
  105.3 28.8 %copy-start.6 = (bf16[128,64]{0,1:T(8,128)(2,1)S(1)}, bf16[128,64]{0,1:T(8,128)(2,1)}, u32[]{:S(2)}) copy-start(bf16[128,64]{0,1:T(8,128)(2,1)} %param.38) | copy-start | bytes 49156
  123.2 51.7 %copy-start.12 = (f32[16,2]{0,1:T(2,128)S(1)}, f32[16,2]{0,1:T(2,128)}, u32[]{:S(2)}) copy-start(f32[16,2]{0,1:T(2,128)} %param.42) | copy-start | bytes 388
  123.2 51.8 %all-to-all-start.2 = ((bf16[32,2,2048]{2,1,0:T(2,128)(2,1)}), bf16[32,2,2048]{2,1,0:T(2,128)(2,1)S(1)}, u32[]{:S(2)}, u32[]{:S(2)}) async-start(bf16[32,2,2048]{2,1,0:T(2,128)(2,1)} %reshape.216), calls=%async_computation.2 | async-start | bytes 524288 | tf_op jit(solution)/shard_map/all_to_all | solution.py:171
  133.2 72.6 %all-gather.6.cloned.1.call-start = ((), (), s32[]{:S(2)}) async-start(), calls=%async_computation.6 | async-start | bytes 1081344 | tf_op jit(solution)/shard_map/all_gather | solution.py:15
  134.0 41.0 %copy-start.2 = (bf16[1,2048,128]{2,1,0:T(8,128)(2,1)S(1)}, bf16[1,2048,128]{2,1,0:T(8,128)(2,1)}, u32[]{:S(2)}) copy-start(bf16[1,2048,128]{2,1,0:T(8,128)(2,1)} %param.43) | copy-start | bytes 1572868
  175.1 1.5 copy-start.3
  175.1 13.4 %copy-start.14 = (f32[16]{0:T(128)S(1)}, f32[16]{0:T(128)}, u32[]{:S(2)}) copy-start(f32[16]{0:T(128)} %param.41) | copy-start | bytes 196
  177.8 33.2 %all-to-all-start.3 = ((bf16[32,2,2048]{2,1,0:T(2,128)(2,1)}), bf16[32,2,2048]{2,1,0:T(2,128)(2,1)S(1)}, u32[]{:S(2)}, u32[]{:S(2)}) async-start(bf16[32,2,2048]{2,1,0:T(2,128)(2,1)} %copy.64), calls=%async_computation.3 | async-start | bytes 524288 | tf_op jit(solution)/shard_map/all_to_all | solution.py:178
Sparse Core Ops, SparseCore 0:
  9.5 81.8 all-gather.3
  136.2 69.6 all-gather.5
where the time goes:
time: 241 us; the launch traced here: 240 us
  waiting for transfers between devices  100 us (41%)
  blocking collectives  59.3 us (25%)
  starting transfers between devices  44.1 us (18%)
  between operations  14.4 us (6%)
  matrix products  10.6 us (4%)
  local copies, waits for them, and re-layouts  6.76 us (3%)
  other arithmetic  4.7 us (2%)
    all_gather x2, waiting for transfers between devices, sent_together(): filled = lax.all_gather(both, axis, axis=dim, tiled=True)  80.8 us
    all_gather x2, blocking collectives, gather_in_order(): pieces = lax.all_gather(pieces, axes[k], axis=0, tiled=True)  40.6 us
    all_to_all x2, starting transfers between devices, from_everyone(): return lax.all_to_all(copies, axis, split_axis=0, concat_axis=0, tiled=True)  23.3 us
    all_to_all x1, blocking collectives, from_everyone(): return lax.all_to_all(copies, axis, split_axis=0, concat_axis=0, tiled=True)  18.7 us
    all_to_all x2, waiting for transfers between devices, from_everyone(): return lax.all_to_all(copies, axis, split_axis=0, concat_axis=0, tiled=True)  15.7 us
    all_to_all x1, starting transfers between devices, shards(): lax.all_to_all(partial_out.reshape(sources, slots_now, feature).astype(jn...  10.6 us
    all_to_all x1, starting transfers between devices, shards(): lax.all_to_all(outbound, EP, split_axis=0, concat_axis=0, tiled=True)  10.1 us
  transfers between devices with their start and end apart: 6, of which 4 were waited for; matrix products, arithmetic and copies ran while one was open for 5% of the time, Pallas kernels for 0%

commit v1 on v0

--- a/solution.py
+++ b/solution.py
@@ -40,7 +40,9 @@
 def gather_in_order(array, axes, sequence):
     pieces = array[None]
     for k in sequence:
-        pieces = lax.all_gather(pieces, axes[k], axis=0, tiled=True)
+        pieces = jnp.concatenate(
+            lax.all_to_all(jnp.stack([pieces] * lax.axis_size(axes[k])), axes[k], 0, 0), axis=0
+        )
     held = [lax.axis_size(axes[k]) for k in reversed(sequence)]
     pieces = pieces.reshape(*held, *array.shape)
     turned = sorted(range(len(sequence)), key=lambda place: sequence[len(sequence) - 1 - place])

time: 241 us -> 265 us (1.100)
  waiting for transfers between devices: 100 us -> 153 us
  blocking collectives: 59.3 us -> 22.4 us
  starting transfers between devices: 44.1 us -> 50.6 us
    all_gather x2 -> x0, blocking collectives: 40.6 us -> none  [gather_in_order(): pieces = lax.all_gather(pieces, axes[k], axis=0, tiled=True)]
    all_gather x2, waiting for transfers between devices: 80.8 us -> 105 us  [sent_together(): filled = lax.all_gather(both, axis, axis=dim, tiled=True)]
    all_to_all x1, waiting for transfers between devices: 0.01 us -> 20.6 us  [shards(): lax.all_to_all(outbound, EP, split_axis=0, concat_axis=0, tiled=True)]
    all_to_all x0 -> x2, starting transfers between devices: none -> 11.3 us  [gather_in_order(): lax.all_to_all(jnp.stack([pieces] * lax.axis_size(axes[k])), axes[k], 0, 0)]
    all_to_all x0 -> x2, waiting for transfers between devices: none -> 11.2 us  [gather_in_order(): lax.all_to_all(jnp.stack([pieces] * lax.axis_size(axes[k])), axes[k], 0, 0)]
    all_to_all x1, starting transfers between devices: 10.6 us -> 3.65 us  [shards(): lax.all_to_all(partial_out.reshape(sources, slots_now, feature).astype(jn...]
    all_to_all x1, waiting for transfers between devices: 3.85 us -> 0.01 us  [shards(): lax.all_to_all(partial_out.reshape(sources, slots_now, feature).astype(jn...]
    all_to_all x1, blocking collectives: 18.7 us -> 22.4 us  [from_everyone(): return lax.all_to_all(copies, axis, split_axis=0, concat_axis=0, tiled=True)]
  transfers between devices with their start and end apart: 6 -> 8, of which waited for: 4 -> 5; matrix products, arithmetic and copies ran while one was open for 5% -> 6% of each run, Pallas kernels for 0% -> 0%
where the time goes in v1:
time: 265 us; the launch traced here: 264 us
  waiting for transfers between devices  153 us (58%)
  starting transfers between devices  50.6 us (19%)
  blocking collectives  22.4 us (8%)
  between operations  14.4 us (5%)
  matrix products  10.6 us (4%)
  local copies, waits for them, and re-layouts  7.3 us (3%)
  other arithmetic  5.54 us (2%)
    all_gather x2, waiting for transfers between devices, sent_together(): filled = lax.all_gather(both, axis, axis=dim, tiled=True)  105 us
    all_to_all x2, starting transfers between devices, from_everyone(): return lax.all_to_all(copies, axis, split_axis=0, concat_axis=0, tiled=True)  23.1 us
    all_to_all x1, blocking collectives, from_everyone(): return lax.all_to_all(copies, axis, split_axis=0, concat_axis=0, tiled=True)  22.4 us
    all_to_all x1, waiting for transfers between devices, shards(): lax.all_to_all(outbound, EP, split_axis=0, concat_axis=0, tiled=True)  20.6 us
    all_to_all x2, waiting for transfers between devices, from_everyone(): return lax.all_to_all(copies, axis, split_axis=0, concat_axis=0, tiled=True)  15.7 us
    all_to_all x1, starting transfers between devices, shards(): lax.all_to_all(outbound, EP, split_axis=0, concat_axis=0, tiled=True)  12.4 us
    all_to_all x2, starting transfers between devices, gather_in_order(): lax.all_to_all(jnp.stack([pieces] * lax.axis_size(axes[k])), axes[k], 0, 0)  11.3 us
    all_to_all x2, waiting for transfers between devices, gather_in_order(): lax.all_to_all(jnp.stack([pieces] * lax.axis_size(axes[k])), axes[k], 0, 0)  11.2 us
  transfers between devices with their start and end apart: 8, of which 5 were waited for; matrix products, arithmetic and copies ran while one was open for 6% of the time, Pallas kernels for 0%

profile of v1, /device:TPU:1, one launch (start us, length us, event | category | flops | bytes accessed | tf_op | source)
XLA Modules:
  0.0 263.8 jit_solution(5826213617477435574)
XLA Ops:
  6.6 1.5 pad_maximum_fusion.1
  8.1 1.6 broadcast_in_dim.15
  9.8 16.7 %all-to-all-start = ((bf16[32,128,64]{1,2,0:T(8,128)(2,1)}), bf16[32,128,64]{1,2,0:T(8,128)(2,1)S(1)}, u32[]{:S(2)}, u32[]{:S(2)}) async-start(bf16[32,128,64]{1,2,0:T(8,128)(2,1)} %broadcast_in_dim.15), calls=%async_computation | async-start | bytes 1048576 | tf_op jit(solution)/shard_map/all_to_all | solution.py:21
  27.8 63.7 %all-gather.3.cloned.1.call-done = bf16[2048,384]{1,0:T(8,128)(2,1)} async-done(((bf16[64,384]{1,0:T(8,128)(2,1)}), bf16[2048,384]{1,0:T(8,128)(2,1)}) %all-gather.3.cloned.1.call-update) | async-done | bytes 1572880 | tf_op jit(solution)/shard_map/all_gather | solution.py:15
  91.5 1.4 convolution_convert_fusion.5
  92.9 1.4 fusion.14
  96.1 1.5 convolution_convert_fusion.2
  97.7 1.1 broadcast_in_dim.16
  98.8 6.4 %all-to-all-start.1 = ((bf16[16,16,2048]{2,1,0:T(8,128)(2,1)}), bf16[16,16,2048]{2,1,0:T(8,128)(2,1)S(1)}, u32[]{:S(2)}, u32[]{:S(2)}) async-start(bf16[16,16,2048]{2,1,0:T(8,128)(2,1)} %broadcast_in_dim.16), calls=%async_computation.1 | async-start | bytes 2097152 | tf_op jit(solution)/shard_map/all_to_all | solution.py:21
  105.8 15.7 %all-to-all-done.1 = bf16[16,16,2048]{2,1,0:T(8,128)(2,1)S(1)} async-done(((bf16[16,16,2048]{2,1,0:T(8,128)(2,1)}), bf16[16,16,2048]{2,1,0:T(8,128)(2,1)S(1)}, u32[]{:S(2)}, u32[]{:S(2)}) %all-to-all-start.1) | async-done | bytes 1048608 | tf_op jit(solution)/shard_map/all_to_all | solution.py:21
  122.3 7.2 %all-to-all-start.4 = ((bf16[16,1,128,64]{2,3,1,0:T(8,128)(2,1)}), bf16[16,1,128,64]{2,3,1,0:T(8,128)(2,1)S(1)}, u32[]{:S(2)}, u32[]{:S(2)}) async-start(bf16[16,1,128,64]{2,3,1,0:T(8,128)(2,1)} %stack.6), calls=%async_computation.4 | async-start | bytes 524288 | tf_op jit(solution)/shard_map/all_to_all | solution.py:44
  130.2 0.9 reshape.215
  131.1 11.2 %all-to-all-done.4 = bf16[16,1,128,64]{2,3,1,0:T(8,128)(2,1)S(1)} async-done(((bf16[16,1,128,64]{2,3,1,0:T(8,128)(2,1)}), bf16[16,1,128,64]{2,3,1,0:T(8,128)(2,1)S(1)}, u32[]{:S(2)}, u32[]{:S(2)}) %all-to-all-start.4) | async-done | bytes 262176 | tf_op jit(solution)/shard_map/all_to_all | solution.py:44
  142.3 12.4 %all-to-all-start.2 = ((bf16[32,2,2048]{2,1,0:T(2,128)(2,1)}), bf16[32,2,2048]{2,1,0:T(2,128)(2,1)S(1)}, u32[]{:S(2)}, u32[]{:S(2)}) async-start(bf16[32,2,2048]{2,1,0:T(2,128)(2,1)} %reshape.215), calls=%async_computation.2 | async-start | bytes 524288 | tf_op jit(solution)/shard_map/all_to_all | solution.py:173
  155.5 0.8 pad_maximum_fusion
  156.4 20.6 %all-to-all-done.2 = bf16[32,2,2048]{2,1,0:T(2,128)(2,1)S(1)} async-done(((bf16[32,2,2048]{2,1,0:T(2,128)(2,1)}), bf16[32,2,2048]{2,1,0:T(2,128)(2,1)S(1)}, u32[]{:S(2)}, u32[]{:S(2)}) %all-to-all-start.2) | async-done | bytes 262176 | tf_op jit(solution)/shard_map/all_to_all | solution.py:173
  177.0 4.1 %all-to-all-start.5 = ((bf16[2,16,128,64]{2,3,1,0:T(8,128)(2,1)}), bf16[2,16,128,64]{2,3,1,0:T(8,128)(2,1)S(1)}, u32[]{:S(2)}, u32[]{:S(2)}) async-start(bf16[2,16,128,64]{2,3,1,0:T(8,128)(2,1)} %pad_maximum_fusion), calls=%async_computation.5 | async-start | bytes 1048576 | tf_op jit(solution)/shard_map/all_to_all | solution.py:44
  181.5 1.3 fusion.6
  183.0 1.0 copy.50
  183.9 3.7 %all-to-all-start.3 = ((bf16[32,2,2048]{2,1,0:T(2,128)(2,1)}), bf16[32,2,2048]{2,1,0:T(2,128)(2,1)S(1)}, u32[]{:S(2)}, u32[]{:S(2)}) async-start(bf16[32,2,2048]{2,1,0:T(2,128)(2,1)} %copy.50), calls=%async_computation.3 | async-start | bytes 524288 | tf_op jit(solution)/shard_map/all_to_all | solution.py:180
  187.9 41.7 %all-gather.5.cloned.1.call-done = bf16[2048,256]{1,0:T(8,128)(2,1)} async-done(((bf16[64,256]{1,0:T(8,128)(2,1)}), bf16[2048,256]{1,0:T(8,128)(2,1)}) %all-gather.5.cloned.1.call-update) | async-done | bytes 1048592 | tf_op jit(solution)/shard_map/all_gather | solution.py:15
  229.6 1.3 fusion.23
  232.2 1.5 fusion.1
  233.8 22.4 %all_to_all.35 = bf16[16,16,2048]{2,1,0:T(8,128)(2,1)S(1)} all-to-all(bf16[16,16,2048]{2,1,0:T(8,128)(2,1)S(1)} %broadcast_in_dim.17), channel_id=1, replica_groups=mesh['ep_0'=16,'ep_1'=2,'tp'=16] {'tp'}, dimensions={0} | all-to-all | bytes 2097152 | tf_op jit(solution)/shard_map/all_to_all | solution.py:21
  (84 shorter events, 8.3 us)
Async XLA Ops:
  6.5 87.8 %copy-start = (bf16[16,1,384,128]{3,2,1,0:T(8,128)(2,1)S(1)}, bf16[16,1,384,128]{3,2,1,0:T(8,128)(2,1)}, u32[]{:S(2)}) copy-start(bf16[16,1,384,128]{3,2,1,0:T(8,128)(2,1)} %param.30) | copy-start | bytes 4718596
  6.5 20.6 %copy-start.1 = (bf16[16,2048]{1,0:T(8,128)(2,1)S(1)}, bf16[16,2048]{1,0:T(8,128)(2,1)}, u32[]{:S(2)}) copy-start(bf16[16,2048]{1,0:T(8,128)(2,1)} %param.23) | copy-start | bytes 196612
  6.5 20.7 %copy-start.13 = (s32[16]{0:T(128)S(1)}, s32[16]{0:T(128)}, u32[]{:S(2)}) copy-start(s32[16]{0:T(128)} %param.33) | copy-start | bytes 196
  6.5 20.8 %copy-start.4 = (f32[16,1,384]{2,1,0:T(1,128)S(1)}, f32[16,1,384]{2,1,0:T(1,128)}, u32[]{:S(2)}) copy-start(f32[16,1,384]{2,1,0:T(1,128)} %param.32) | copy-start | bytes 73732
  6.5 21.1 %copy-start.9 = (f32[2048]{0:T(1024)S(1)}, f32[2048]{0:T(1024)}, u32[]{:S(2)}) copy-start(f32[2048]{0:T(1024)} %param.24) | copy-start | bytes 24580
  6.5 21.1 %copy-start.16 = (bf16[2048,1]{0,1:T(2,128)(2,1)S(1)}, bf16[2048,1]{0,1:T(2,128)(2,1)}, u32[]{:S(2)}) copy-start(bf16[2048,1]{0,1:T(2,128)(2,1)} %param.28) | copy-start | bytes 12292
  6.6 85.0 %all-gather.3.cloned.1.call-start = ((), (), s32[]{:S(2)}) async-start(), calls=%async_computation.7 | async-start | bytes 1622016 | tf_op jit(solution)/shard_map/all_gather | solution.py:15
  9.8 86.4 %all-to-all-start = ((bf16[32,128,64]{1,2,0:T(8,128)(2,1)}), bf16[32,128,64]{1,2,0:T(8,128)(2,1)S(1)}, u32[]{:S(2)}, u32[]{:S(2)}) async-start(bf16[32,128,64]{1,2,0:T(8,128)(2,1)} %broadcast_in_dim.15), calls=%async_computation | async-start | bytes 1048576 | tf_op jit(solution)/shard_map/all_to_all | solution.py:21
  91.5 4.2 %copy-start.15 = (bf16[16,1,384,128]{3,2,1,0:T(8,128)(2,1)S(1)}, bf16[16,1,384,128]{3,2,1,0:T(8,128)(2,1)}, u32[]{:S(2)}) copy-start(bf16[16,1,384,128]{3,2,1,0:T(8,128)(2,1)} %param.31) | copy-start | bytes 4718596
  97.6 7.5 %copy-start.11 = (s32[16,2]{0,1:T(2,128)S(1)}, s32[16,2]{0,1:T(2,128)}, u32[]{:S(2)}) copy-start(s32[16,2]{0,1:T(2,128)} %param.40) | copy-start | bytes 388
  97.6 23.9 %copy-start.6 = (bf16[128,64]{0,1:T(8,128)(2,1)S(1)}, bf16[128,64]{0,1:T(8,128)(2,1)}, u32[]{:S(2)}) copy-start(bf16[128,64]{0,1:T(8,128)(2,1)} %param.38) | copy-start | bytes 49156
  98.8 22.8 %all-to-all-start.1 = ((bf16[16,16,2048]{2,1,0:T(8,128)(2,1)}), bf16[16,16,2048]{2,1,0:T(8,128)(2,1)S(1)}, u32[]{:S(2)}, u32[]{:S(2)}) async-start(bf16[16,16,2048]{2,1,0:T(8,128)(2,1)} %broadcast_in_dim.16), calls=%async_computation.1 | async-start | bytes 2097152 | tf_op jit(solution)/shard_map/all_to_all | solution.py:21
  105.2 24.7 %copy-start.5 = (f32[2048]{0:T(1024)S(1)}, f32[2048]{0:T(1024)}, u32[]{:S(2)}) copy-start(f32[2048]{0:T(1024)} %param.35) | copy-start | bytes 24580
  122.3 32.4 %copy-start.7 = (bf16[64,128]{1,0:T(8,128)(2,1)S(1)}, bf16[64,128]{1,0:T(8,128)(2,1)}, u32[]{:S(2)}) copy-start(bf16[64,128]{1,0:T(8,128)(2,1)} %param.37) | copy-start | bytes 49156
  122.3 32.4 %copy-start.8 = (bf16[64,128]{1,0:T(8,128)(2,1)S(1)}, bf16[64,128]{1,0:T(8,128)(2,1)}, u32[]{:S(2)}) copy-start(bf16[64,128]{1,0:T(8,128)(2,1)} %param.36) | copy-start | bytes 49156
  122.3 19.9 %all-to-all-start.4 = ((bf16[16,1,128,64]{2,3,1,0:T(8,128)(2,1)}), bf16[16,1,128,64]{2,3,1,0:T(8,128)(2,1)S(1)}, u32[]{:S(2)}, u32[]{:S(2)}) async-start(bf16[16,1,128,64]{2,3,1,0:T(8,128)(2,1)} %stack.6), calls=%async_computation.4 | async-start | bytes 524288 | tf_op jit(solution)/shard_map/all_to_all | solution.py:44
  129.5 25.9 %copy-start.10 = (bf16[2048]{0:T(1024)(128)(2,1)S(1)}, bf16[2048]{0:T(1024)(128)(2,1)}, u32[]{:S(2)}) copy-start(bf16[2048]{0:T(1024)(128)(2,1)} %param.39) | copy-start | bytes 12292
  129.6 25.9 %copy-start.12 = (f32[16,2]{0,1:T(2,128)S(1)}, f32[16,2]{0,1:T(2,128)}, u32[]{:S(2)}) copy-start(f32[16,2]{0,1:T(2,128)} %param.42) | copy-start | bytes 388
  131.1 50.1 %copy-start.2 = (bf16[1,2048,128]{2,1,0:T(8,128)(2,1)S(1)}, bf16[1,2048,128]{2,1,0:T(8,128)(2,1)}, u32[]{:S(2)}) copy-start(bf16[1,2048,128]{2,1,0:T(8,128)(2,1)} %param.43) | copy-start | bytes 1572868
  142.3 34.7 %all-to-all-start.2 = ((bf16[32,2,2048]{2,1,0:T(2,128)(2,1)}), bf16[32,2,2048]{2,1,0:T(2,128)(2,1)S(1)}, u32[]{:S(2)}, u32[]{:S(2)}) async-start(bf16[32,2,2048]{2,1,0:T(2,128)(2,1)} %reshape.215), calls=%async_computation.2 | async-start | bytes 524288 | tf_op jit(solution)/shard_map/all_to_all | solution.py:173
  154.7 74.9 %all-gather.5.cloned.1.call-start = ((), (), s32[]{:S(2)}) async-start(), calls=%async_computation.8 | async-start | bytes 1081344 | tf_op jit(solution)/shard_map/all_gather | solution.py:15
  177.0 7.0 %all-to-all-start.5 = ((bf16[2,16,128,64]{2,3,1,0:T(8,128)(2,1)}), bf16[2,16,128,64]{2,3,1,0:T(8,128)(2,1)S(1)}, u32[]{:S(2)}, u32[]{:S(2)}) async-start(bf16[2,16,128,64]{2,3,1,0:T(8,128)(2,1)} %pad_maximum_fusion), calls=%async_computation.5 | async-start | bytes 1048576 | tf_op jit(solution)/shard_map/all_to_all | solution.py:44
  181.2 6.4 %copy-start.14 = (f32[16]{0:T(128)S(1)}, f32[16]{0:T(128)}, u32[]{:S(2)}) copy-start(f32[16]{0:T(128)} %param.41) | copy-start | bytes 196
  183.9 46.9 %all-to-all-start.3 = ((bf16[32,2,2048]{2,1,0:T(2,128)(2,1)}), bf16[32,2,2048]{2,1,0:T(2,128)(2,1)S(1)}, u32[]{:S(2)}, u32[]{:S(2)}) async-start(bf16[32,2,2048]{2,1,0:T(2,128)(2,1)} %copy.50), calls=%async_computation.3 | async-start | bytes 524288 | tf_op jit(solution)/shard_map/all_to_all | solution.py:180
  (1 other events, 1.5 us)
Sparse Core Ops, SparseCore 0:
  9.5 81.9 all-gather.2
  157.6 71.9 all-gather.4
